TPU v7x, 128 devices: a whole 4x4x4 slice. The times are simulated.
128 devices in a mesh: sp: 16 (over z, y), dp: 8 (over x, core).
Axes of the slice: x: 4, y: 4, z: 4, core: 2. Of those that a mesh axis runs over, the one named last changes fastest.
Arguments:
- residual: bfloat16 [8, 4096, 2048], P('dp', 'sp'), may hold values from -6 to 6
- queries: bfloat16 [8, 4096, 1024], P('dp', 'sp'), may hold values from -400 to 400
- key_vectors: bfloat16 [8, 4096, 1024], P('dp', 'sp'), may hold values from -6 to 6
- value_vectors: bfloat16 [8, 4096, 1024], P('dp', 'sp'), may hold values from -6 to 6
- gate_cache: float32 [8, 4096, 16], P('dp', 'sp'), may hold values from -514 to 0, as said below
- out_weight: bfloat16 [1024, 2048], P(None, 'dp'), may hold values from -0.1875 to 0.1875
- mix_gain: float32 [2048], replicated, may hold values from 0.1 to 1.9
- route_gain: float32 [2048], replicated, may hold values from 0.1 to 1.9
- out_gain: float32 [2048], replicated, may hold values from 0.1 to 1.9
- routes: int32 [8, 4096, 2], P('dp', 'sp'), may hold values from 0 to 15, all different within a row; in each aligned block of 256 rows (0 to 255, 256 to 511, ..., all dimensions but the last counted through in order) at most 64 rows name the same one
- group_share: float32 [8, 4096], P('dp', 'sp'), may hold values from 0.2 to 1
- expert_share: float32 [8, 4096, 2], P('dp', 'sp'), may hold values from 0.1 to 1
- gate_proj: bfloat16 [16, 2048, 1024], P('sp'), may hold values from -0.125 to 0.125
- up_proj: bfloat16 [16, 2048, 1024], P('sp'), may hold values from -0.125 to 0.125
- down_proj: bfloat16 [16, 1024, 2048], P('sp'), may hold values from -0.1875 to 0.1875
Outputs:
- layer_out: bfloat16 [8, 4096, 2048], P('dp', 'sp')
Inputs may be any that keep to these rules, and one draw needn't show every extreme that they name: `gate_cache`: along the positions of a sequence the values never rise. `routes`: the 2 experts of a position differ. Within the rows of one device (aligned blocks of 256 positions) no expert is named more than 64 times, a bound that some block reaches.
All inputs are finite; a program needn't handle non-finite values.
Results may differ from a plain program's by a relative error of at most 0.0085.
Values may be sent and summed in bfloat16 or wider, within the bound.
No kernel may reach another device: no remote copies, remote signals or barrier semaphores. Data moves between devices by JAX's collectives and lax.ppermute only.
A program may use at most 128 MiB of HBM per device.

v0:
```python
import jax
import jax.numpy as jnp
from jax import lax
from jax.experimental import pallas as pl
from jax.experimental.pallas import tpu as pltpu
from jax.sharding import PartitionSpec as P


F32 = jnp.float32
BF16 = jnp.bfloat16
HD = 64
SLOTS = 64
NEG = -1e30


def vmem(mib):
    return pltpu.CompilerParams(vmem_limit_bytes=mib * 1024 * 1024)


def vspec():
    return pl.BlockSpec(memory_space=pltpu.VMEM)


def hspec():
    return pl.BlockSpec(memory_space=pltpu.HBM)


def pack_kernel(q_hbm, k_hbm, v_hbm, g_ref, o_hbm, q_ref, k_ref, v_ref, o_ref, in_sem, out_sem):
    rows = q_ref.shape[0]
    half = rows // 2
    heads = g_ref.shape[0]
    groups = out_sem.shape[0]
    step = heads // groups
    loads = []
    for part in range(2):
        for i, (src, dst) in enumerate(((q_hbm, q_ref), (k_hbm, k_ref), (v_hbm, v_ref))):
            cols = slice(512 * part, 512 * part + 512)
            loads.append(pltpu.make_async_copy(
                src.at[0, :, cols], dst.at[:, cols], in_sem.at[3 * part + i]))
            loads[-1].start()
    gates = g_ref[...]
    hi = gates.astype(BF16).astype(F32)
    mid = (gates - hi).astype(BF16).astype(F32)
    low = gates - hi - mid
    stores = []
    for pair in range(heads // 2):
        if pair % 4 == 0:
            for c in loads[3 * (pair // 4):3 * (pair // 4) + 3]:
                c.wait()
        cols = slice(128 * pair, 128 * pair + 128)
        q, k, v = q_ref[:, cols], k_ref[:, cols], v_ref[:, cols]
        for side in range(2):
            h = 2 * pair + side
            at = slice(64 * side, 64 * side + 64)
            o_ref[h, 0:rows, :] = jnp.concatenate([q[:, at], k[:, at]], axis=1)
            o_ref[h, rows:rows + half, :] = jnp.concatenate([v[:half, at], v[half:, at]], axis=1)
            terms = [t[h:h + 1, 128 * j:128 * j + 128] for t in (hi, mid, low) for j in range(2)]
            terms.append(jnp.zeros((10, 128), F32))
            o_ref[h, rows + half:rows + half + 16, :] = jnp.concatenate(terms, axis=0).astype(BF16)
        if (2 * pair + 2) % step == 0:
            g = (2 * pair + 2) // step - 1
            at = slice(g * step, (g + 1) * step)
            stores.append(pltpu.make_async_copy(o_ref.at[at], o_hbm.at[at], out_sem.at[g]))
            stores[-1].start()
    for c in stores:
        c.wait()


def pack(q, k, v, g):
    heads, rows = g.shape
    shape = (heads, rows + rows // 2 + 16, 128)
    return pl.pallas_call(
        pack_kernel,
        out_shape=jax.ShapeDtypeStruct(shape, BF16),
        in_specs=[hspec()] * 3 + [vspec()],
        out_specs=hspec(),
        scratch_shapes=[pltpu.VMEM(q.shape[1:], BF16)] * 3 + [
            pltpu.VMEM(shape, BF16),
            pltpu.SemaphoreType.DMA((6,)),
            pltpu.SemaphoreType.DMA((4,)),
        ],
        compiler_params=vmem(63),
        name="pack",
    )(q, k, v, g)


TILE = 512


def attend_kernel(x_ref, o_ref, q_scr, k_scr, v_scr, buf_a, buf_b):
    blocks = x_ref.shape[0]
    rows = (x_ref.shape[1] - 16) * 2 // 3
    half = rows // 2
    lane = lax.broadcasted_iota(jnp.int32, (rows, 64), 1)
    minus = jnp.where(lane < 3, -1.0, 0.0).astype(BF16)
    ones = jnp.where(lane < 1, 1.0, 0.0).astype(BF16)
    pr = lax.broadcasted_iota(jnp.int32, (16, 128), 0)
    pc = lax.broadcasted_iota(jnp.int32, (16, 128), 1)
    picks = [
        jnp.where((pr == 2 * (pc - 64) + j) & (pc >= 64) & (pc < 67), 1.0, 0.0).astype(BF16)
        for j in range(2)
    ]
    nt = (((1,), (1,)), ((), ()))
    tn = (((0,), (0,)), ((), ()))

    def prepare(b):
        base = b * rows
        qk = x_ref[b, 0:rows, :]
        q = (qk[:, 0:64].astype(F32) * (HD ** -0.5)).astype(BF16)
        q_scr[base:base + rows, :] = jnp.concatenate([q, minus], axis=1)
        terms = x_ref[b, rows + half:rows + half + 16, :]
        for j in range(2):
            ext = lax.dot_general(terms, picks[j], tn, preferred_element_type=F32).astype(BF16)
            at = slice(half * j, half * j + half)
            k_scr[base + half * j:base + half * j + half, :] = jnp.concatenate(
                [qk[at, 64:128], ext[:, 64:128]], axis=1)
        v = x_ref[b, rows:rows + half, :]
        v_scr[base:base + half, :] = jnp.concatenate([v[:, 0:64], ones[:half]], axis=1)
        v_scr[base + half:base + rows, :] = jnp.concatenate([v[:, 64:128], ones[:half]], axis=1)

    def score(q0, qn, k0, kn):
        return lax.dot_general(
            q_scr[q0:q0 + qn, :], k_scr[k0:k0 + kn, :], nt, preferred_element_type=F32)

    def top_of(s, m=None):
        for j in range(s.shape[1] // 128):
            t = s[:, 128 * j:128 * j + 128]
            m = t if m is None else jnp.maximum(m, t)
        return m

    def masked(s, off):
        r = lax.broadcasted_iota(jnp.int32, s.shape, 0) + off
        c = lax.broadcasted_iota(jnp.int32, s.shape, 1)
        return jnp.where(c <= r, s, NEG)

    hq = TILE // 2

    def scores_of(qi, buf):
        q0, m = qi * TILE, None
        for k0 in range(0, q0, TILE):
            s = score(q0, TILE, k0, TILE)
            buf[:, k0:k0 + TILE] = s
            m = top_of(s, m)
            yield m
        s1 = masked(score(q0, hq, q0, hq), 0)
        s2 = masked(score(q0 + hq, hq, q0, TILE), hq)
        buf[0:hq, q0:q0 + hq] = s1
        buf[hq:TILE, q0:q0 + TILE] = s2
        d = jnp.concatenate([top_of(s1), top_of(s2)], axis=0)
        yield d if m is None else jnp.maximum(m, d)

    def mix_of(qi, buf, m):
        q0 = qi * TILE
        acc = jnp.zeros((TILE, 128), F32)
        for k0 in range(0, q0, TILE):
            p = jnp.exp(buf[:, k0:k0 + TILE] - m).astype(BF16)
            acc = acc + jnp.dot(p, v_scr[k0:k0 + TILE, :], preferred_element_type=F32)
            yield acc
        p1 = jnp.exp(buf[0:hq, q0:q0 + hq] - m[0:hq]).astype(BF16)
        p2 = jnp.exp(buf[hq:TILE, q0:q0 + TILE] - m[hq:]).astype(BF16)
        a1 = jnp.dot(p1, v_scr[q0:q0 + hq, :], preferred_element_type=F32)
        a2 = jnp.dot(p2, v_scr[q0:q0 + TILE, :], preferred_element_type=F32)
        yield acc + jnp.concatenate([a1, a2], axis=0)

    per = TILE // rows

    def store(qi, acc):
        out = acc[:, 0:64] * (1.0 / acc[:, 64:65])
        for j in range(per):
            top = out[j * rows:j * rows + half]
            bottom = out[j * rows + half:(j + 1) * rows]
            o_ref[per * qi + j] = jnp.concatenate([top, bottom], axis=1).astype(BF16)

    n = blocks // per
    bufs = [buf_a, buf_b]
    m_old = None
    for qi in range(n + 1):
        first, second = iter(()), iter(())
        if qi < n:
            for b in range(per):
                prepare(qi * per + b)
            first = scores_of(qi, bufs[qi % 2])
        if qi:
            second = mix_of(qi - 1, bufs[(qi - 1) % 2], m_old)
        m = acc = None
        while True:
            a, b = next(first, None), next(second, None)
            if a is None and b is None:
                break
            m = m if a is None else a
            acc = acc if b is None else b
        if m is not None:
            m_old = jnp.max(m, axis=1, keepdims=True)
        if acc is not None:
            store(qi - 1, acc)


def attend(x):
    blocks = x.shape[0]
    rows = (x.shape[1] - 16) * 2 // 3
    length = blocks * rows
    return pl.pallas_call(
        attend_kernel,
        out_shape=jax.ShapeDtypeStruct((blocks, rows // 2, 128), BF16),
        in_specs=[vspec()],
        out_specs=vspec(),
        scratch_shapes=[
            pltpu.VMEM((length, 128), BF16),
            pltpu.VMEM((length, 128), BF16),
            pltpu.VMEM((length, 128), BF16),
            pltpu.VMEM((TILE, length), F32),
            pltpu.VMEM((TILE, length), F32),
        ],
        compiler_params=pltpu.CompilerParams(vmem_limit_bytes=54000000),
        cost_estimate=pl.CostEstimate(
            flops=4 * length * length * 64, transcendentals=length * length // 2, bytes_accessed=4000000),
        name="attend",
    )(x)


def route_kernel(r_ref, gs_ref, es_ref, p_ref, c_ref):
    rows = r_ref.shape[1]
    experts = p_ref.shape[0]
    fill = jnp.zeros((3, rows), F32)
    columns = jnp.concatenate([r_ref[...].astype(F32), gs_ref[...], es_ref[...], fill], axis=0)
    columns = jnp.concatenate([columns, jnp.zeros((120, rows), F32)], axis=0).T
    e0, e1 = columns[:, 0:1].astype(jnp.int32), columns[:, 1:2].astype(jnp.int32)
    lane = lax.broadcasted_iota(jnp.int32, (rows, 128), 1)
    named = jnp.where((lane == e0) | (lane == e1), 1.0, 0.0)
    ri = lax.broadcasted_iota(jnp.int32, (rows, rows), 0)
    ci = lax.broadcasted_iota(jnp.int32, (rows, rows), 1)
    before = jnp.where(ci < ri, 1.0, 0.0).astype(BF16)
    rank = jnp.dot(before, named.astype(BF16), preferred_element_type=F32)
    p_ref[...] = jnp.where(named > 0, rank, -1.0).T[:experts]
    share, s0, s1 = columns[:, 2:3], columns[:, 3:4], columns[:, 4:5]
    total = s0 + s1
    w0, w1 = share * s0 / total, share * s1 / total
    k0 = jnp.sum(jnp.where(lane == e0, rank, 0.0), axis=1, keepdims=True).astype(jnp.int32)
    k1 = jnp.sum(jnp.where(lane == e1, rank, 0.0), axis=1, keepdims=True).astype(jnp.int32)
    at = lax.broadcasted_iota(jnp.int32, (rows, experts * SLOTS), 1)
    w = jnp.where(at == e0 * SLOTS + k0, w0, jnp.where(at == e1 * SLOTS + k1, w1, 0.0))
    c_ref[...] = w.astype(BF16)


def route_tables(routes, group_share, expert_share, experts):
    rows = routes.shape[1]
    n = experts * SLOTS
    return pl.pallas_call(
        route_kernel,
        out_shape=(jax.ShapeDtypeStruct((experts, rows), F32), jax.ShapeDtypeStruct((rows, n), BF16)),
        in_specs=[vspec()] * 3,
        out_specs=(vspec(),) * 2,
        compiler_params=vmem(12),
        name="route_tables",
    )(routes, group_share, expert_share)


def project_kernel(*refs):
    shards = len(refs) - 12
    here_ref, a_ref = refs[0:2]
    w_refs = refs[2:2 + shards]
    res_ref, mg_ref, rg_ref, p_ref, hid_ref, out_ref = refs[2 + shards:8 + shards]
    w_scr, mix_scr, p_scr, w_sem = refs[8 + shards:]
    heads, half = a_ref.shape[0], a_ref.shape[1]
    cols = w_scr.shape[2]
    loads = [pltpu.make_async_copy(w_refs[i], w_scr.at[i], w_sem.at[i]) for i in range(shards)]
    for c in loads:
        c.start()
    rows = p_ref.shape[1]
    slot = lax.broadcasted_iota(jnp.int32, (SLOTS, rows), 0).astype(F32)
    for e in range(p_ref.shape[0]):
        p_scr[e * SLOTS:(e + 1) * SLOTS, :] = jnp.where(
            p_ref[e:e + 1, :] == slot, 1.0, 0.0).astype(BF16)
    att = jnp.concatenate([
        jnp.concatenate([
            jnp.concatenate([a_ref[2 * j][:, side], a_ref[2 * j + 1][:, side]], axis=1)
            for j in range(heads // 2)
        ], axis=1)
        for side in (slice(0, 64), slice(64, 128))
    ], axis=0)
    chips = shards // 2
    chip, core = lax.div(here_ref[0], 2), lax.rem(here_ref[0], 2)
    for c in loads:
        c.wait()
    for i in range(shards):
        turn, swapped = i % chips, i // chips
        shard = lax.rem(chip + chips - turn, chips) * 2 + (1 - core if swapped else core)
        at = pl.multiple_of(shard * cols, cols)
        mix_scr[:, pl.ds(at, cols)] = jnp.dot(att, w_scr[i], preferred_element_type=F32)
    width = mix_scr.shape[1]
    scales = []
    for part in range(4):
        at = slice(half // 2 * part, half // 2 * (part + 1))
        mixed = mix_scr[at, :]
        scale = lax.rsqrt(jnp.mean(mixed * mixed, axis=1, keepdims=True) + 1e-6)
        hidden = (res_ref[at, :].astype(F32) + mixed * scale * mg_ref[...]).astype(BF16)
        hid_ref[at, :] = hidden
        h = hidden.astype(F32)
        scales.append(lax.rsqrt(jnp.mean(h * h, axis=1, keepdims=True) + 1e-6))
    scale = jnp.concatenate(scales, axis=0)
    for j in range(0, width, 512):
        at = slice(j, j + 512)
        routed = (hid_ref[:, at].astype(F32) * scale * rg_ref[:, at]).astype(BF16)
        out_ref[:, at] = jnp.dot(p_scr[...], routed, preferred_element_type=F32).astype(BF16)


def project(here, att, weights, residual, mix_gain, route_gain, table):
    rows, width = residual.shape
    n = len(weights)
    return pl.pallas_call(
        project_kernel,
        out_shape=(
            jax.ShapeDtypeStruct((rows, width), BF16),
            jax.ShapeDtypeStruct((table.shape[0] * SLOTS, width), BF16),
        ),
        in_specs=[pl.BlockSpec(memory_space=pltpu.SMEM), vspec()] + [hspec()] * n + [vspec()] * 4,
        out_specs=(vspec(), vspec()),
        scratch_shapes=[
            pltpu.VMEM((n,) + weights[0].shape, BF16),
            pltpu.VMEM((rows, width), F32),
            pltpu.VMEM((table.shape[0] * SLOTS, rows), BF16),
            pltpu.SemaphoreType.DMA((n,)),
        ],
        compiler_params=vmem(42),
        name="project",
    )(here, att, *weights, residual, mix_gain, route_gain, table)


def expert_kernel(x_ref, g_ref, u_ref, d_ref, o_ref, act_scr):
    ft, dt = 512, 512

    def hidden(f, _):
        at = pl.ds(pl.multiple_of(f * ft, ft), ft)
        gate = jnp.dot(x_ref[...], g_ref[:, at], preferred_element_type=F32)
        upper = jnp.dot(x_ref[...], u_ref[:, at], preferred_element_type=F32)
        act_scr[:, at] = (gate / (1.0 + jnp.exp(-gate)) * upper).astype(BF16)
        return 0

    lax.fori_loop(0, act_scr.shape[1] // ft, hidden, 0)

    def result(j, _):
        at = pl.ds(pl.multiple_of(j * dt, dt), dt)
        o_ref[:, at] = jnp.dot(act_scr[...], d_ref[:, at], preferred_element_type=F32).astype(BF16)
        return 0

    lax.fori_loop(0, o_ref.shape[1] // dt, result, 0)


def expert(x, gate, up, down):
    rows, width = x.shape
    ff = gate.shape[1]
    return pl.pallas_call(
        expert_kernel,
        out_shape=jax.ShapeDtypeStruct((rows, width), BF16),
        in_specs=[vspec()] * 4,
        out_specs=vspec(),
        scratch_shapes=[pltpu.VMEM((rows, ff), BF16)],
        compiler_params=vmem(26),
        cost_estimate=pl.CostEstimate(
            flops=6 * rows * width * ff, transcendentals=rows * ff, bytes_accessed=20000000),
        name="expert",
    )(x, gate, up, down)


def finish_kernel(c_ref, x_ref, hid_ref, og_ref, o_ref, o_scr, o_sem):
    n, _, ct = o_scr.shape
    stores = [
        pltpu.make_async_copy(o_scr.at[j], o_ref.at[:, j * ct:(j + 1) * ct], o_sem.at[j])
        for j in range(n)
    ]
    for j in range(n):
        at = slice(j * ct, (j + 1) * ct)
        combined = jnp.dot(c_ref[...], x_ref[:, at], preferred_element_type=F32)
        o_scr[j] = (hid_ref[:, at].astype(F32) + combined * og_ref[:, at]).astype(BF16)
        stores[j].start()
    for c in stores:
        c.wait()


def finish(table, x, hidden, out_gain, ct=512):
    rows, width = hidden.shape
    n = width // ct
    return pl.pallas_call(
        finish_kernel,
        out_shape=jax.ShapeDtypeStruct(hidden.shape, BF16),
        in_specs=[vspec()] * 4,
        out_specs=hspec(),
        scratch_shapes=[pltpu.VMEM((n, rows, ct), BF16), pltpu.SemaphoreType.DMA((n,))],
        compiler_params=vmem(16),
        name="finish",
    )(table, x, hidden, out_gain)


def swap(x):
    return lax.all_to_all(x, "sp", split_axis=0, concat_axis=0, tiled=True)


def gather_shards(x):
    n = lax.axis_size("dp")
    chips = n // 2
    own = [x]
    for k in range(1, chips):
        own.append(
            lax.ppermute(x, "dp", [(d, (d // 2 + k) % chips * 2 + d % 2) for d in range(n)]))
    other = [lax.ppermute(t, "dp", [(d, d ^ 1) for d in range(n)]) for t in own]
    return own + other, lax.axis_index("dp").astype(jnp.int32)[None]


def layer(
    residual,
    queries,
    key_vectors,
    value_vectors,
    gate_cache,
    out_weight,
    mix_gain,
    route_gain,
    out_gain,
    routes,
    group_share,
    expert_share,
    gate_proj,
    up_proj,
    down_proj,
):
    experts = lax.axis_size("sp")
    width = residual.shape[2]
    weights, here = gather_shards(out_weight)
    packed = pack(queries, key_vectors, value_vectors, gate_cache[0].T)
    arrived = swap(packed)
    table, back = route_tables(routes[0].T, group_share, expert_share[0].T, experts)
    attended = attend(arrived)
    att = swap(attended)
    hidden, rows_out = project(
        here, att, weights, residual[0], mix_gain[None], route_gain[None], table)

    def exchange(x):
        return swap(x.reshape(experts, SLOTS, width)).reshape(x.shape)

    result = expert(exchange(rows_out), gate_proj[0], up_proj[0], down_proj[0])
    return finish(back, exchange(result), hidden, out_gain[None])[None]


def solution(mesh):
    placed = (
        P("dp", "sp", None),
        P("dp", "sp", None),
        P("dp", "sp", None),
        P("dp", "sp", None),
        P("dp", "sp", None),
        P(None, "dp"),
        P(),
        P(),
        P(),
        P("dp", "sp", None),
        P("dp", "sp"),
        P("dp", "sp", None),
        P("sp", None, None),
        P("sp", None, None),
        P("sp", None, None),
    )
    return jax.shard_map(
        layer, mesh=mesh, in_specs=placed, out_specs=P("dp", "sp", None), check_vma=False
    )
```

profile of v0, /device:TPU:0, one launch (start us, length us, event | category | flops | bytes accessed | tf_op | source)
XLA Modules:
  0.0 201.7 jit_solution(3539680766785251855)
XLA Ops:
  0.0 3.4 %pack.1 = bf16[16,400,128]{2,1,0:T(8,128)(2,1)} custom-call(bf16[1,256,1024]{2,1,0:T(8,128)(2,1)} %q_hbm.1, bf16[1,256,1024]{2,1,0:T(8,128)(2,1)} %k_hbm.1, bf16[1,256,1024]{2,1,0:T(8,128)(2,1)} %v_hbm.1, f32[16,256]{1,0:T(8,128)} %bitcast.35), custom_call_target="tpu_custom_call" | custom-call | tf_op jit(solution)/shard_map/pack/pallas_call | solution.py:72
  3.4 8.2 %all-to-all-start = ((bf16[16,400,128]{2,1,0:T(8,128)(2,1)}), bf16[16,400,128]{2,1,0:T(8,128)(2,1)S(1)}, u32[]{:S(2)}, u32[]{:S(2)}) async-start(bf16[16,400,128]{2,1,0:T(8,128)(2,1)} %pack.1), calls=%async_computation | async-start | bytes 3276800 | tf_op jit(solution)/shard_map/all_to_all | solution.py:395
  11.6 0.0 copy-start.8
  11.6 0.0 copy-start
  11.6 0.0 copy-start.4
  11.6 2.8 %collective-permute-start.2 = (bf16[1024,256]{1,0:T(8,128)(2,1)S(1)}, bf16[1024,256]{1,0:T(8,128)(2,1)}, u32[]{:S(2)}, u32[]{:S(2)}) collective-permute-start(bf16[1024,256]{1,0:T(8,128)(2,1)S(1)} %copy-done.1), channel_id=1, source_target_pairs={{0,6},{1,7},{2,0},{3,1},{4,2},{5,3},{6,4},{7,5},{8,14},{9,15},{10,... | collective-permute-start | bytes 1572872 | tf_op jit(solution)/shard_map/ppermute | solution.py:404
  14.5 0.8 collective-permute-start.1
  15.3 0.9 collective-permute-start
  16.2 20.5 %collective-permute-done.2.refs_5_ = bf16[1024,256]{1,0:T(8,128)(2,1)} collective-permute-done((bf16[1024,256]{1,0:T(8,128)(2,1)S(1)}, bf16[1024,256]{1,0:T(8,128)(2,1)}, u32[]{:S(2)}, u32[]{:S(2)}) %collective-permute-start.2) | collective-permute-done | bytes 524320 | tf_op jit(solution)/shard_map/ppermute | solution.py:404
  36.6 0.5 collective-permute-start.5
  37.2 3.3 %collective-permute-done.refs_3_ = bf16[1024,256]{1,0:T(8,128)(2,1)} collective-permute-done((bf16[1024,256]{1,0:T(8,128)(2,1)S(1)}, bf16[1024,256]{1,0:T(8,128)(2,1)}, u32[]{:S(2)}, u32[]{:S(2)}) %collective-permute-start) | collective-permute-done | bytes 524320 | tf_op jit(solution)/shard_map/ppermute | solution.py:404
  40.4 0.0 collective-permute-start.4
  40.4 11.8 %attend.1 = bf16[16,128,128]{2,1,0:T(8,128)(2,1)S(1)} custom-call(bf16[16,400,128]{2,1,0:T(8,128)(2,1)S(1)} %all-to-all-done.x_ref), custom_call_target="tpu_custom_call" | custom-call | flops 4294967296 | bytes 4000000 | tf_op jit(solution)/shard_map/attend/pallas_call | solution.py:202
  52.2 0.0 copy-start.2
  52.2 0.8 copy-done.2
  53.0 7.2 %all-to-all-start.1 = ((bf16[16,128,128]{2,1,0:T(8,128)(2,1)}), bf16[16,128,128]{2,1,0:T(8,128)(2,1)S(1)}, u32[]{:S(2)}, u32[]{:S(2)}) async-start(bf16[16,128,128]{2,1,0:T(8,128)(2,1)} %copy-done.2), calls=%async_computation.1 | async-start | bytes 1048576 | tf_op jit(solution)/shard_map/all_to_all | solution.py:395
  60.2 1.1 route_tables.1
  61.4 11.0 %all-to-all-done.1.refs_1_ = bf16[16,128,128]{2,1,0:T(8,128)(2,1)S(1)} async-done(((bf16[16,128,128]{2,1,0:T(8,128)(2,1)}), bf16[16,128,128]{2,1,0:T(8,128)(2,1)S(1)}, u32[]{:S(2)}, u32[]{:S(2)}) %all-to-all-start.1) | async-done | bytes 524320 | tf_op jit(solution)/shard_map/all_to_all | solution.py:395
  72.4 5.6 %project.1 = (bf16[256,2048]{1,0:T(8,128)(2,1)S(1)}, bf16[1024,2048]{1,0:T(8,128)(2,1)S(1)}) custom-call(s32[1]{0:T(128)} %bitcast.4.refs_0_, bf16[16,128,128]{2,1,0:T(8,128)(2,1)S(1)} %all-to-all-done.1.refs_1_, bf16[1024,256]{1,0:T(8,128)(2,1)S(1)} %copy-done.1, bf16[1024,256]{1,0:T(8,128)(2,1)} %collective-permute-done.refs_3_, ...), custom_call_target="tpu_custom_call" | custom-call | tf_op jit(solution)/shard_map/project/pallas_call | solution.py:310
  78.1 0.0 copy-start.9
  78.1 53.7 %all_to_all.20 = bf16[16,64,2048]{2,1,0:T(8,128)(2,1)S(1)} all-to-all(bf16[16,64,2048]{2,1,0:T(8,128)(2,1)S(1)} %bitcast.23), channel_id=1, replica_groups=mesh['sp'=16,'dp'=8] {'sp'}, dimensions={0} | all-to-all | bytes 8388608 | tf_op jit(solution)/shard_map/all_to_all | solution.py:395
  131.8 14.1 %expert.1 = bf16[1024,2048]{1,0:T(8,128)(2,1)S(1)} custom-call(bf16[1024,2048]{1,0:T(8,128)(2,1)S(1)} %bitcast.24, bf16[2048,1024]{1,0:T(8,128)(2,1)S(1)} %bitcast.32, bf16[2048,1024]{1,0:T(8,128)(2,1)S(1)} %bitcast.33, bf16[1024,2048]{1,0:T(8,128)(2,1)S(1)} %bitcast.34), custom_call_target="tpu_custom_call" | custom-call | flops 12884901888 | bytes 20000000 | tf_op jit(solution)/shard_map/expert/pallas_call | solution.py:352
  145.9 53.6 %all_to_all.21 = bf16[16,64,2048]{2,1,0:T(8,128)(2,1)S(1)} all-to-all(bf16[16,64,2048]{2,1,0:T(8,128)(2,1)S(1)} %bitcast.25), channel_id=1, replica_groups=mesh['sp'=16,'dp'=8] {'sp'}, dimensions={0} | all-to-all | bytes 8388608 | tf_op jit(solution)/shard_map/all_to_all | solution.py:395
  199.5 2.0 finish.1
  (26 shorter events, 0.1 us)
Async XLA Ops:
  0.0 11.6 %copy-start.1 = (bf16[1024,256]{1,0:T(8,128)(2,1)S(1)}, bf16[1024,256]{1,0:T(8,128)(2,1)}, u32[]{:S(2)}) copy-start(bf16[1024,256]{1,0:T(8,128)(2,1)} %refs_2_.1) | copy-start | bytes 1572868
  3.4 37.1 %all-to-all-start = ((bf16[16,400,128]{2,1,0:T(8,128)(2,1)}), bf16[16,400,128]{2,1,0:T(8,128)(2,1)S(1)}, u32[]{:S(2)}, u32[]{:S(2)}) async-start(bf16[16,400,128]{2,1,0:T(8,128)(2,1)} %pack.1), calls=%async_computation | async-start | bytes 3276800 | tf_op jit(solution)/shard_map/all_to_all | solution.py:395
  11.6 48.6 %copy-start.6 = (s32[1,256,2]{1,2,0:T(2,128)S(1)}, s32[1,256,2]{1,2,0:T(2,128)}, u32[]{:S(2)}) copy-start(s32[1,256,2]{1,2,0:T(2,128)} %param.24) | copy-start | bytes 6148
  11.6 48.6 %copy-start.7 = (f32[1,256,2]{1,2,0:T(2,128)S(1)}, f32[1,256,2]{1,2,0:T(2,128)}, u32[]{:S(2)}) copy-start(f32[1,256,2]{1,2,0:T(2,128)} %param.26) | copy-start | bytes 6148
  11.6 48.6 %copy-start.8 = (f32[1,256]{1,0:T(1,128)S(1)}, f32[1,256]{1,0:T(1,128)}, u32[]{:S(2)}) copy-start(f32[1,256]{1,0:T(1,128)} %gs_ref.1) | copy-start | bytes 3076
  11.6 60.8 %copy-start = (bf16[1,256,2048]{2,1,0:T(8,128)(2,1)S(1)}, bf16[1,256,2048]{2,1,0:T(8,128)(2,1)}, u32[]{:S(2)}) copy-start(bf16[1,256,2048]{2,1,0:T(8,128)(2,1)} %param.15) | copy-start | bytes 3145732
  11.6 60.8 %copy-start.3 = (f32[2048]{0:T(1024)S(1)}, f32[2048]{0:T(1024)}, u32[]{:S(2)}) copy-start(f32[2048]{0:T(1024)} %param.21) | copy-start | bytes 24580
  11.6 60.8 %copy-start.4 = (f32[2048]{0:T(1024)S(1)}, f32[2048]{0:T(1024)}, u32[]{:S(2)}) copy-start(f32[2048]{0:T(1024)} %param.22) | copy-start | bytes 24580
  11.6 25.0 %collective-permute-start.2 = (bf16[1024,256]{1,0:T(8,128)(2,1)S(1)}, bf16[1024,256]{1,0:T(8,128)(2,1)}, u32[]{:S(2)}, u32[]{:S(2)}) collective-permute-start(bf16[1024,256]{1,0:T(8,128)(2,1)S(1)} %copy-done.1), channel_id=1, source_target_pairs={{0,6},{1,7},{2,0},{3,1},{4,2},{5,3},{6,4},{7,5},{8,14},{9,15},{10,... | collective-permute-start | bytes 1572872 | tf_op jit(solution)/shard_map/ppermute | solution.py:404
  14.5 22.2 %collective-permute-start.1 = (bf16[1024,256]{1,0:T(8,128)(2,1)S(1)}, bf16[1024,256]{1,0:T(8,128)(2,1)}, u32[]{:S(2)}, u32[]{:S(2)}) collective-permute-start(bf16[1024,256]{1,0:T(8,128)(2,1)S(1)} %copy-done.1), channel_id=1, source_target_pairs={{0,4},{1,5},{2,6},{3,7},{4,0},{5,1},{6,2},{7,3},{8,12},{9,13},{10,... | collective-permute-start | bytes 1572872 | tf_op jit(solution)/shard_map/ppermute | solution.py:404
  15.3 25.1 %collective-permute-start = (bf16[1024,256]{1,0:T(8,128)(2,1)S(1)}, bf16[1024,256]{1,0:T(8,128)(2,1)}, u32[]{:S(2)}, u32[]{:S(2)}) collective-permute-start(bf16[1024,256]{1,0:T(8,128)(2,1)S(1)} %copy-done.1), channel_id=1, source_target_pairs={{0,2},{1,3},{2,4},{3,5},{4,6},{5,7},{6,0},{7,1},{8,10},{9,11},{10,... | collective-permute-start | bytes 1572872 | tf_op jit(solution)/shard_map/ppermute | solution.py:404
  16.2 45.2 %collective-permute-start.3 = (bf16[1024,256]{1,0:T(8,128)(2,1)S(1)}, bf16[1024,256]{1,0:T(8,128)(2,1)}, u32[]{:S(2)}, u32[]{:S(2)}) collective-permute-start(bf16[1024,256]{1,0:T(8,128)(2,1)S(1)} %copy-done.1), channel_id=1, source_target_pairs={{0,1},{1,0},{2,3},{3,2},{4,5},{5,4},{6,7},{7,6},{8,9},{9,8},{10,11... | collective-permute-start | bytes 1572872 | tf_op jit(solution)/shard_map/ppermute | solution.py:405
  36.6 24.7 %collective-permute-start.6 = (bf16[1024,256]{1,0:T(8,128)(2,1)}, bf16[1024,256]{1,0:T(8,128)(2,1)}, u32[]{:S(2)}, u32[]{:S(2)}) collective-permute-start(bf16[1024,256]{1,0:T(8,128)(2,1)} %collective-permute-done.2.refs_5_), channel_id=1, source_target_pairs={{0,1},{1,0},{2,3},{3,2},{4,5},{5,4},{6,7},{7,6},{8,9},{9,8},{10,11... | collective-permute-start | bytes 1572872 | tf_op jit(solution)/shard_map/ppermute | solution.py:405
  36.6 24.7 %collective-permute-start.5 = (bf16[1024,256]{1,0:T(8,128)(2,1)}, bf16[1024,256]{1,0:T(8,128)(2,1)}, u32[]{:S(2)}, u32[]{:S(2)}) collective-permute-start(bf16[1024,256]{1,0:T(8,128)(2,1)} %collective-permute-done.1.refs_4_), channel_id=1, source_target_pairs={{0,1},{1,0},{2,3},{3,2},{4,5},{5,4},{6,7},{7,6},{8,9},{9,8},{10,11... | collective-permute-start | bytes 1572872 | tf_op jit(solution)/shard_map/ppermute | solution.py:405
  40.4 20.9 %collective-permute-start.4 = (bf16[1024,256]{1,0:T(8,128)(2,1)}, bf16[1024,256]{1,0:T(8,128)(2,1)}, u32[]{:S(2)}, u32[]{:S(2)}) collective-permute-start(bf16[1024,256]{1,0:T(8,128)(2,1)} %collective-permute-done.refs_3_), channel_id=1, source_target_pairs={{0,1},{1,0},{2,3},{3,2},{4,5},{5,4},{6,7},{7,6},{8,9},{9,8},{10,11... | collective-permute-start | bytes 1572872 | tf_op jit(solution)/shard_map/ppermute | solution.py:405
  52.2 0.8 copy-start.2
  53.0 19.4 %all-to-all-start.1 = ((bf16[16,128,128]{2,1,0:T(8,128)(2,1)}), bf16[16,128,128]{2,1,0:T(8,128)(2,1)S(1)}, u32[]{:S(2)}, u32[]{:S(2)}) async-start(bf16[16,128,128]{2,1,0:T(8,128)(2,1)} %copy-done.2), calls=%async_computation.1 | async-start | bytes 1048576 | tf_op jit(solution)/shard_map/all_to_all | solution.py:395
  72.4 59.4 %copy-start.11 = (bf16[1,1024,2048]{2,1,0:T(8,128)(2,1)S(1)}, bf16[1,1024,2048]{2,1,0:T(8,128)(2,1)}, u32[]{:S(2)}) copy-start(bf16[1,1024,2048]{2,1,0:T(8,128)(2,1)} %param.29) | copy-start | bytes 12582916
  78.1 53.7 %copy-start.9 = (bf16[1,2048,1024]{2,1,0:T(8,128)(2,1)S(1)}, bf16[1,2048,1024]{2,1,0:T(8,128)(2,1)}, u32[]{:S(2)}) copy-start(bf16[1,2048,1024]{2,1,0:T(8,128)(2,1)} %param.27) | copy-start | bytes 12582916
  78.1 53.7 %copy-start.10 = (bf16[1,2048,1024]{2,1,0:T(8,128)(2,1)S(1)}, bf16[1,2048,1024]{2,1,0:T(8,128)(2,1)}, u32[]{:S(2)}) copy-start(bf16[1,2048,1024]{2,1,0:T(8,128)(2,1)} %param.28) | copy-start | bytes 12582916
  145.9 53.6 %copy-start.5 = (f32[2048]{0:T(1024)S(1)}, f32[2048]{0:T(1024)}, u32[]{:S(2)}) copy-start(f32[2048]{0:T(1024)} %param.23) | copy-start | bytes 24580
where the time goes:
time: 202 us
  blocking collectives  107 us (53%)
  Pallas kernels  38 us (19%)
  waiting for transfers between devices  34.8 us (17%)
  starting transfers between devices  20.4 us (10%)
    all_to_all x2, blocking collectives, swap(): return lax.all_to_all(x, 'sp', split_axis=0, concat_axis=0, tiled=True)  107 us
    ppermute x3, waiting for transfers between devices, gather_shards(): lax.ppermute(x, 'dp', [(d, (d // 2 + k) % chips * 2 + d % 2) for d in ran...  23.7 us
    all_to_all x2, starting transfers between devices, swap(): return lax.all_to_all(x, 'sp', split_axis=0, concat_axis=0, tiled=True)  15.3 us
    pallas_call x1, Pallas kernels, expert(): pl.pallas_call(expert_kernel, out_shape=jax.ShapeDtypeStruct((rows, width...  14.1 us
    pallas_call x1, Pallas kernels, attend(): pl.pallas_call(attend_kernel, out_shape=jax.ShapeDtypeStruct((blocks, row...  11.8 us
    all_to_all x2, waiting for transfers between devices, swap(): return lax.all_to_all(x, 'sp', split_axis=0, concat_axis=0, tiled=True)  11 us
    pallas_call x1, Pallas kernels, project(): pl.pallas_call(project_kernel, out_shape=(jax.ShapeDtypeStruct((rows, wid...  5.65 us
    ppermute x3, starting transfers between devices, gather_shards(): lax.ppermute(x, 'dp', [(d, (d // 2 + k) % chips * 2 + d % 2) for d in ran...  4.51 us
  transfers between devices with their start and end apart: 9, of which 3 were waited for; matrix products, arithmetic and copies ran while one was open for 0% of the time, Pallas kernels for 6%

commit v1 on v0

--- a/solution.py
+++ b/solution.py
@@ -25,12 +25,15 @@
     return pl.BlockSpec(memory_space=pltpu.HBM)
 
 
-def pack_kernel(q_hbm, k_hbm, v_hbm, g_ref, o_hbm, q_ref, k_ref, v_ref, o_ref, in_sem, out_sem):
+def pack_kernel(q_hbm, k_hbm, v_hbm, g_hbm, o_hbm, q_ref, k_ref, v_ref, g_ref, o_ref, in_sem, g_sem,
+                out_sem):
     rows = q_ref.shape[0]
     half = rows // 2
     heads = g_ref.shape[0]
     groups = out_sem.shape[0]
     step = heads // groups
+    gate_load = pltpu.make_async_copy(g_hbm, g_ref, g_sem)
+    gate_load.start()
     loads = []
     for part in range(2):
         for i, (src, dst) in enumerate(((q_hbm, q_ref), (k_hbm, k_ref), (v_hbm, v_ref))):
@@ -38,6 +41,7 @@
             loads.append(pltpu.make_async_copy(
                 src.at[0, :, cols], dst.at[:, cols], in_sem.at[3 * part + i]))
             loads[-1].start()
+    gate_load.wait()
     gates = g_ref[...]
     hi = gates.astype(BF16).astype(F32)
     mid = (gates - hi).astype(BF16).astype(F32)
@@ -72,11 +76,13 @@
     return pl.pallas_call(
         pack_kernel,
         out_shape=jax.ShapeDtypeStruct(shape, BF16),
-        in_specs=[hspec()] * 3 + [vspec()],
+        in_specs=[hspec()] * 4,
         out_specs=hspec(),
         scratch_shapes=[pltpu.VMEM(q.shape[1:], BF16)] * 3 + [
+            pltpu.VMEM(g.shape, F32),
             pltpu.VMEM(shape, BF16),
             pltpu.SemaphoreType.DMA((6,)),
+            pltpu.SemaphoreType.DMA,
             pltpu.SemaphoreType.DMA((4,)),
         ],
         compiler_params=vmem(63),
@@ -85,6 +91,7 @@
 
 
 TILE = 512
+CHUNK = 1024
 
 
 def attend_kernel(x_ref, o_ref, q_scr, k_scr, v_scr, buf_a, buf_b):
@@ -137,9 +144,10 @@
 
     def scores_of(qi, buf):
         q0, m = qi * TILE, None
-        for k0 in range(0, q0, TILE):
-            s = score(q0, TILE, k0, TILE)
-            buf[:, k0:k0 + TILE] = s
+        for k0 in range(0, q0, CHUNK):
+            kn = min(CHUNK, q0 - k0)
+            s = score(q0, TILE, k0, kn)
+            buf[:, k0:k0 + kn] = s
             m = top_of(s, m)
             yield m
         s1 = masked(score(q0, hq, q0, hq), 0)
@@ -152,9 +160,10 @@
     def mix_of(qi, buf, m):
         q0 = qi * TILE
         acc = jnp.zeros((TILE, 128), F32)
-        for k0 in range(0, q0, TILE):
-            p = jnp.exp(buf[:, k0:k0 + TILE] - m).astype(BF16)
-            acc = acc + jnp.dot(p, v_scr[k0:k0 + TILE, :], preferred_element_type=F32)
+        for k0 in range(0, q0, CHUNK):
+            at = slice(k0, min(k0 + CHUNK, q0))
+            p = jnp.exp(buf[:, at] - m).astype(BF16)
+            acc = acc + jnp.dot(p, v_scr[at, :], preferred_element_type=F32)
             yield acc
         p1 = jnp.exp(buf[0:hq, q0:q0 + hq] - m[0:hq]).astype(BF16)
         p2 = jnp.exp(buf[hq:TILE, q0:q0 + TILE] - m[hq:]).astype(BF16)

time: 202 us -> 201 us (level)
  no operation moved by 1% of the time
where the time goes in v1:
time: 201 us; the launch traced here: 200 us
  blocking collectives  107 us (53%)
  Pallas kernels  37 us (18%)
  waiting for transfers between devices  34.8 us (17%)
  starting transfers between devices  20.2 us (10%)
    all_to_all x2, blocking collectives, swap(): return lax.all_to_all(x, 'sp', split_axis=0, concat_axis=0, tiled=True)  107 us
    ppermute x3, waiting for transfers between devices, gather_shards(): lax.ppermute(x, 'dp', [(d, (d // 2 + k) % chips * 2 + d % 2) for d in ran...  23.7 us
    all_to_all x2, starting transfers between devices, swap(): return lax.all_to_all(x, 'sp', split_axis=0, concat_axis=0, tiled=True)  15.1 us
    pallas_call x1, Pallas kernels, expert(): pl.pallas_call(expert_kernel, out_shape=jax.ShapeDtypeStruct((rows, width...  14.1 us
    pallas_call x1, Pallas kernels, attend(): pl.pallas_call(attend_kernel, out_shape=jax.ShapeDtypeStruct((blocks, row...  11.5 us
    all_to_all x2, waiting for transfers between devices, swap(): return lax.all_to_all(x, 'sp', split_axis=0, concat_axis=0, tiled=True)  11 us
    pallas_call x1, Pallas kernels, project(): pl.pallas_call(project_kernel, out_shape=(jax.ShapeDtypeStruct((rows, wid...  5.64 us
    ppermute x3, starting transfers between devices, gather_shards(): lax.ppermute(x, 'dp', [(d, (d // 2 + k) % chips * 2 + d % 2) for d in ran...  4.51 us
  transfers between devices with their start and end apart: 9, of which 3 were waited for; matrix products, arithmetic and copies ran while one was open for 0% of the time, Pallas kernels for 6%

profile of v1, /device:TPU:0, one launch (start us, length us, event | category | flops | bytes accessed | tf_op | source)
XLA Modules:
  0.0 200.5 jit_solution(9876940718979769767)
XLA Ops:
  0.0 2.7 %pack.1 = bf16[16,400,128]{2,1,0:T(8,128)(2,1)} custom-call(bf16[1,256,1024]{2,1,0:T(8,128)(2,1)} %q_hbm.1, bf16[1,256,1024]{2,1,0:T(8,128)(2,1)} %k_hbm.1, bf16[1,256,1024]{2,1,0:T(8,128)(2,1)} %v_hbm.1, f32[16,256]{1,0:T(8,128)} %bitcast.35), custom_call_target="tpu_custom_call" | custom-call | tf_op jit(solution)/shard_map/pack/pallas_call | solution.py:76
  2.7 8.2 %all-to-all-start = ((bf16[16,400,128]{2,1,0:T(8,128)(2,1)}), bf16[16,400,128]{2,1,0:T(8,128)(2,1)S(1)}, u32[]{:S(2)}, u32[]{:S(2)}) async-start(bf16[16,400,128]{2,1,0:T(8,128)(2,1)} %pack.1), calls=%async_computation | async-start | bytes 3276800 | tf_op jit(solution)/shard_map/all_to_all | solution.py:404
  10.9 0.0 copy-start.7
  10.9 0.0 copy-start.8
  10.9 0.0 copy-start.4
  11.0 2.8 %collective-permute-start.2 = (bf16[1024,256]{1,0:T(8,128)(2,1)S(1)}, bf16[1024,256]{1,0:T(8,128)(2,1)}, u32[]{:S(2)}, u32[]{:S(2)}) collective-permute-start(bf16[1024,256]{1,0:T(8,128)(2,1)S(1)} %copy-done.1), channel_id=1, source_target_pairs={{0,6},{1,7},{2,0},{3,1},{4,2},{5,3},{6,4},{7,5},{8,14},{9,15},{10,... | collective-permute-start | bytes 1572872 | tf_op jit(solution)/shard_map/ppermute | solution.py:413
  13.8 0.8 collective-permute-start.1
  14.6 0.9 collective-permute-start
  15.5 20.5 %collective-permute-done.2.refs_5_ = bf16[1024,256]{1,0:T(8,128)(2,1)} collective-permute-done((bf16[1024,256]{1,0:T(8,128)(2,1)S(1)}, bf16[1024,256]{1,0:T(8,128)(2,1)}, u32[]{:S(2)}, u32[]{:S(2)}) %collective-permute-start.2) | collective-permute-done | bytes 524320 | tf_op jit(solution)/shard_map/ppermute | solution.py:413
  36.0 0.5 collective-permute-start.5
  36.5 3.3 %collective-permute-done.refs_3_ = bf16[1024,256]{1,0:T(8,128)(2,1)} collective-permute-done((bf16[1024,256]{1,0:T(8,128)(2,1)S(1)}, bf16[1024,256]{1,0:T(8,128)(2,1)}, u32[]{:S(2)}, u32[]{:S(2)}) %collective-permute-start) | collective-permute-done | bytes 524320 | tf_op jit(solution)/shard_map/ppermute | solution.py:413
  39.7 0.0 collective-permute-start.4
  39.7 11.5 %attend.1 = bf16[16,128,128]{2,1,0:T(8,128)(2,1)S(1)} custom-call(bf16[16,400,128]{2,1,0:T(8,128)(2,1)S(1)} %all-to-all-done.x_ref), custom_call_target="tpu_custom_call" | custom-call | flops 4294967296 | bytes 4000000 | tf_op jit(solution)/shard_map/attend/pallas_call | solution.py:211
  51.3 0.8 copy-done.2
  52.0 6.9 %all-to-all-start.1 = ((bf16[16,128,128]{2,1,0:T(8,128)(2,1)}), bf16[16,128,128]{2,1,0:T(8,128)(2,1)S(1)}, u32[]{:S(2)}, u32[]{:S(2)}) async-start(bf16[16,128,128]{2,1,0:T(8,128)(2,1)} %copy-done.2), calls=%async_computation.1 | async-start | bytes 1048576 | tf_op jit(solution)/shard_map/all_to_all | solution.py:404
  59.0 1.1 route_tables.1
  60.2 11.0 %all-to-all-done.1.refs_1_ = bf16[16,128,128]{2,1,0:T(8,128)(2,1)S(1)} async-done(((bf16[16,128,128]{2,1,0:T(8,128)(2,1)}), bf16[16,128,128]{2,1,0:T(8,128)(2,1)S(1)}, u32[]{:S(2)}, u32[]{:S(2)}) %all-to-all-start.1) | async-done | bytes 524320 | tf_op jit(solution)/shard_map/all_to_all | solution.py:404
  71.2 0.0 copy-start.11
  71.2 5.6 %project.1 = (bf16[256,2048]{1,0:T(8,128)(2,1)S(1)}, bf16[1024,2048]{1,0:T(8,128)(2,1)S(1)}) custom-call(s32[1]{0:T(128)} %bitcast.4.refs_0_, bf16[16,128,128]{2,1,0:T(8,128)(2,1)S(1)} %all-to-all-done.1.refs_1_, bf16[1024,256]{1,0:T(8,128)(2,1)S(1)} %copy-done.1, bf16[1024,256]{1,0:T(8,128)(2,1)} %collective-permute-done.refs_3_, ...), custom_call_target="tpu_custom_call" | custom-call | tf_op jit(solution)/shard_map/project/pallas_call | solution.py:319
  76.9 53.7 %all_to_all.20 = bf16[16,64,2048]{2,1,0:T(8,128)(2,1)S(1)} all-to-all(bf16[16,64,2048]{2,1,0:T(8,128)(2,1)S(1)} %bitcast.23), channel_id=1, replica_groups=mesh['sp'=16,'dp'=8] {'sp'}, dimensions={0} | all-to-all | bytes 8388608 | tf_op jit(solution)/shard_map/all_to_all | solution.py:404
  130.6 14.1 %expert.1 = bf16[1024,2048]{1,0:T(8,128)(2,1)S(1)} custom-call(bf16[1024,2048]{1,0:T(8,128)(2,1)S(1)} %bitcast.24, bf16[2048,1024]{1,0:T(8,128)(2,1)S(1)} %bitcast.32, bf16[2048,1024]{1,0:T(8,128)(2,1)S(1)} %bitcast.33, bf16[1024,2048]{1,0:T(8,128)(2,1)S(1)} %bitcast.34), custom_call_target="tpu_custom_call" | custom-call | flops 12884901888 | bytes 20000000 | tf_op jit(solution)/shard_map/expert/pallas_call | solution.py:361
  144.7 0.0 copy-start.5
  144.7 53.6 %all_to_all.21 = bf16[16,64,2048]{2,1,0:T(8,128)(2,1)S(1)} all-to-all(bf16[16,64,2048]{2,1,0:T(8,128)(2,1)S(1)} %bitcast.25), channel_id=1, replica_groups=mesh['sp'=16,'dp'=8] {'sp'}, dimensions={0} | all-to-all | bytes 8388608 | tf_op jit(solution)/shard_map/all_to_all | solution.py:404
  198.3 2.0 %finish.1 = bf16[256,2048]{1,0:T(8,128)(2,1)} custom-call(bf16[256,1024]{1,0:T(8,128)(2,1)S(1)} %get-tuple-element.9.c_ref, bf16[1024,2048]{1,0:T(8,128)(2,1)S(1)} %bitcast.22, bf16[256,2048]{1,0:T(8,128)(2,1)S(1)} %get-tuple-element.12.hid_ref, f32[1,2048]{1,0:T(1,128)S(1)} %bitcast.29), custom_call_target="tpu_custom_call" | custom-call | tf_op jit(solution)/shard_map/finish/pallas_call | solution.py:392
  (26 shorter events, 0.1 us)
Async XLA Ops:
  0.0 10.9 %copy-start.1 = (bf16[1024,256]{1,0:T(8,128)(2,1)S(1)}, bf16[1024,256]{1,0:T(8,128)(2,1)}, u32[]{:S(2)}) copy-start(bf16[1024,256]{1,0:T(8,128)(2,1)} %refs_2_.1) | copy-start | bytes 1572868
  2.7 37.1 %all-to-all-start = ((bf16[16,400,128]{2,1,0:T(8,128)(2,1)}), bf16[16,400,128]{2,1,0:T(8,128)(2,1)S(1)}, u32[]{:S(2)}, u32[]{:S(2)}) async-start(bf16[16,400,128]{2,1,0:T(8,128)(2,1)} %pack.1), calls=%async_computation | async-start | bytes 3276800 | tf_op jit(solution)/shard_map/all_to_all | solution.py:404
  10.9 48.1 %copy-start.6 = (s32[1,256,2]{1,2,0:T(2,128)S(1)}, s32[1,256,2]{1,2,0:T(2,128)}, u32[]{:S(2)}) copy-start(s32[1,256,2]{1,2,0:T(2,128)} %param.24) | copy-start | bytes 6148
  10.9 48.1 %copy-start.7 = (f32[1,256,2]{1,2,0:T(2,128)S(1)}, f32[1,256,2]{1,2,0:T(2,128)}, u32[]{:S(2)}) copy-start(f32[1,256,2]{1,2,0:T(2,128)} %param.26) | copy-start | bytes 6148
  10.9 48.1 %copy-start.8 = (f32[1,256]{1,0:T(1,128)S(1)}, f32[1,256]{1,0:T(1,128)}, u32[]{:S(2)}) copy-start(f32[1,256]{1,0:T(1,128)} %gs_ref.1) | copy-start | bytes 3076
  10.9 60.3 %copy-start = (bf16[1,256,2048]{2,1,0:T(8,128)(2,1)S(1)}, bf16[1,256,2048]{2,1,0:T(8,128)(2,1)}, u32[]{:S(2)}) copy-start(bf16[1,256,2048]{2,1,0:T(8,128)(2,1)} %param.15) | copy-start | bytes 3145732
  10.9 60.3 %copy-start.3 = (f32[2048]{0:T(1024)S(1)}, f32[2048]{0:T(1024)}, u32[]{:S(2)}) copy-start(f32[2048]{0:T(1024)} %param.21) | copy-start | bytes 24580
  10.9 60.3 %copy-start.4 = (f32[2048]{0:T(1024)S(1)}, f32[2048]{0:T(1024)}, u32[]{:S(2)}) copy-start(f32[2048]{0:T(1024)} %param.22) | copy-start | bytes 24580
  11.0 25.0 %collective-permute-start.2 = (bf16[1024,256]{1,0:T(8,128)(2,1)S(1)}, bf16[1024,256]{1,0:T(8,128)(2,1)}, u32[]{:S(2)}, u32[]{:S(2)}) collective-permute-start(bf16[1024,256]{1,0:T(8,128)(2,1)S(1)} %copy-done.1), channel_id=1, source_target_pairs={{0,6},{1,7},{2,0},{3,1},{4,2},{5,3},{6,4},{7,5},{8,14},{9,15},{10,... | collective-permute-start | bytes 1572872 | tf_op jit(solution)/shard_map/ppermute | solution.py:413
  13.8 22.2 %collective-permute-start.1 = (bf16[1024,256]{1,0:T(8,128)(2,1)S(1)}, bf16[1024,256]{1,0:T(8,128)(2,1)}, u32[]{:S(2)}, u32[]{:S(2)}) collective-permute-start(bf16[1024,256]{1,0:T(8,128)(2,1)S(1)} %copy-done.1), channel_id=1, source_target_pairs={{0,4},{1,5},{2,6},{3,7},{4,0},{5,1},{6,2},{7,3},{8,12},{9,13},{10,... | collective-permute-start | bytes 1572872 | tf_op jit(solution)/shard_map/ppermute | solution.py:413
  14.6 25.1 %collective-permute-start = (bf16[1024,256]{1,0:T(8,128)(2,1)S(1)}, bf16[1024,256]{1,0:T(8,128)(2,1)}, u32[]{:S(2)}, u32[]{:S(2)}) collective-permute-start(bf16[1024,256]{1,0:T(8,128)(2,1)S(1)} %copy-done.1), channel_id=1, source_target_pairs={{0,2},{1,3},{2,4},{3,5},{4,6},{5,7},{6,0},{7,1},{8,10},{9,11},{10,... | collective-permute-start | bytes 1572872 | tf_op jit(solution)/shard_map/ppermute | solution.py:413
  15.5 44.7 %collective-permute-start.3 = (bf16[1024,256]{1,0:T(8,128)(2,1)S(1)}, bf16[1024,256]{1,0:T(8,128)(2,1)}, u32[]{:S(2)}, u32[]{:S(2)}) collective-permute-start(bf16[1024,256]{1,0:T(8,128)(2,1)S(1)} %copy-done.1), channel_id=1, source_target_pairs={{0,1},{1,0},{2,3},{3,2},{4,5},{5,4},{6,7},{7,6},{8,9},{9,8},{10,11... | collective-permute-start | bytes 1572872 | tf_op jit(solution)/shard_map/ppermute | solution.py:414
  35.9 24.2 %collective-permute-start.6 = (bf16[1024,256]{1,0:T(8,128)(2,1)}, bf16[1024,256]{1,0:T(8,128)(2,1)}, u32[]{:S(2)}, u32[]{:S(2)}) collective-permute-start(bf16[1024,256]{1,0:T(8,128)(2,1)} %collective-permute-done.2.refs_5_), channel_id=1, source_target_pairs={{0,1},{1,0},{2,3},{3,2},{4,5},{5,4},{6,7},{7,6},{8,9},{9,8},{10,11... | collective-permute-start | bytes 1572872 | tf_op jit(solution)/shard_map/ppermute | solution.py:414
  36.0 24.2 %collective-permute-start.5 = (bf16[1024,256]{1,0:T(8,128)(2,1)}, bf16[1024,256]{1,0:T(8,128)(2,1)}, u32[]{:S(2)}, u32[]{:S(2)}) collective-permute-start(bf16[1024,256]{1,0:T(8,128)(2,1)} %collective-permute-done.1.refs_4_), channel_id=1, source_target_pairs={{0,1},{1,0},{2,3},{3,2},{4,5},{5,4},{6,7},{7,6},{8,9},{9,8},{10,11... | collective-permute-start | bytes 1572872 | tf_op jit(solution)/shard_map/ppermute | solution.py:414
  39.7 20.4 %collective-permute-start.4 = (bf16[1024,256]{1,0:T(8,128)(2,1)}, bf16[1024,256]{1,0:T(8,128)(2,1)}, u32[]{:S(2)}, u32[]{:S(2)}) collective-permute-start(bf16[1024,256]{1,0:T(8,128)(2,1)} %collective-permute-done.refs_3_), channel_id=1, source_target_pairs={{0,1},{1,0},{2,3},{3,2},{4,5},{5,4},{6,7},{7,6},{8,9},{9,8},{10,11... | collective-permute-start | bytes 1572872 | tf_op jit(solution)/shard_map/ppermute | solution.py:414
  51.3 0.8 copy-start.2
  52.0 19.1 %all-to-all-start.1 = ((bf16[16,128,128]{2,1,0:T(8,128)(2,1)}), bf16[16,128,128]{2,1,0:T(8,128)(2,1)S(1)}, u32[]{:S(2)}, u32[]{:S(2)}) async-start(bf16[16,128,128]{2,1,0:T(8,128)(2,1)} %copy-done.2), calls=%async_computation.1 | async-start | bytes 1048576 | tf_op jit(solution)/shard_map/all_to_all | solution.py:404
  71.2 59.4 %copy-start.11 = (bf16[1,1024,2048]{2,1,0:T(8,128)(2,1)S(1)}, bf16[1,1024,2048]{2,1,0:T(8,128)(2,1)}, u32[]{:S(2)}) copy-start(bf16[1,1024,2048]{2,1,0:T(8,128)(2,1)} %param.29) | copy-start | bytes 12582916
  76.9 53.7 %copy-start.9 = (bf16[1,2048,1024]{2,1,0:T(8,128)(2,1)S(1)}, bf16[1,2048,1024]{2,1,0:T(8,128)(2,1)}, u32[]{:S(2)}) copy-start(bf16[1,2048,1024]{2,1,0:T(8,128)(2,1)} %param.27) | copy-start | bytes 12582916
  76.9 53.7 %copy-start.10 = (bf16[1,2048,1024]{2,1,0:T(8,128)(2,1)S(1)}, bf16[1,2048,1024]{2,1,0:T(8,128)(2,1)}, u32[]{:S(2)}) copy-start(bf16[1,2048,1024]{2,1,0:T(8,128)(2,1)} %param.28) | copy-start | bytes 12582916
  144.7 53.6 %copy-start.5 = (f32[2048]{0:T(1024)S(1)}, f32[2048]{0:T(1024)}, u32[]{:S(2)}) copy-start(f32[2048]{0:T(1024)} %param.23) | copy-start | bytes 24580

commit v2 on v0

--- a/solution.py
+++ b/solution.py
@@ -25,12 +25,15 @@
     return pl.BlockSpec(memory_space=pltpu.HBM)
 
 
-def pack_kernel(q_hbm, k_hbm, v_hbm, g_ref, o_hbm, q_ref, k_ref, v_ref, o_ref, in_sem, out_sem):
+def pack_kernel(q_hbm, k_hbm, v_hbm, g_hbm, o_hbm, q_ref, k_ref, v_ref, g_ref, o_ref, in_sem, g_sem,
+                out_sem):
     rows = q_ref.shape[0]
     half = rows // 2
     heads = g_ref.shape[0]
     groups = out_sem.shape[0]
     step = heads // groups
+    gate_load = pltpu.make_async_copy(g_hbm, g_ref, g_sem)
+    gate_load.start()
     loads = []
     for part in range(2):
         for i, (src, dst) in enumerate(((q_hbm, q_ref), (k_hbm, k_ref), (v_hbm, v_ref))):
@@ -38,6 +41,7 @@
             loads.append(pltpu.make_async_copy(
                 src.at[0, :, cols], dst.at[:, cols], in_sem.at[3 * part + i]))
             loads[-1].start()
+    gate_load.wait()
     gates = g_ref[...]
     hi = gates.astype(BF16).astype(F32)
     mid = (gates - hi).astype(BF16).astype(F32)
@@ -72,11 +76,13 @@
     return pl.pallas_call(
         pack_kernel,
         out_shape=jax.ShapeDtypeStruct(shape, BF16),
-        in_specs=[hspec()] * 3 + [vspec()],
+        in_specs=[hspec()] * 4,
         out_specs=hspec(),
         scratch_shapes=[pltpu.VMEM(q.shape[1:], BF16)] * 3 + [
+            pltpu.VMEM(g.shape, F32),
             pltpu.VMEM(shape, BF16),
             pltpu.SemaphoreType.DMA((6,)),
+            pltpu.SemaphoreType.DMA,
             pltpu.SemaphoreType.DMA((4,)),
         ],
         compiler_params=vmem(63),
@@ -377,7 +383,7 @@
         c.wait()
 
 
-def finish(table, x, hidden, out_gain, ct=512):
+def finish(table, x, hidden, out_gain, ct=256):
     rows, width = hidden.shape
     n = width // ct
     return pl.pallas_call(

time: 202 us -> 201 us (level)
  no operation moved by 1% of the time
where the time goes in v2:
time: 201 us
  blocking collectives  107 us (53%)
  Pallas kernels  37.3 us (19%)
  waiting for transfers between devices  34.8 us (17%)
  starting transfers between devices  20.4 us (10%)
    all_to_all x2, blocking collectives, swap(): return lax.all_to_all(x, 'sp', split_axis=0, concat_axis=0, tiled=True)  107 us
    ppermute x3, waiting for transfers between devices, gather_shards(): lax.ppermute(x, 'dp', [(d, (d // 2 + k) % chips * 2 + d % 2) for d in ran...  23.7 us
    all_to_all x2, starting transfers between devices, swap(): return lax.all_to_all(x, 'sp', split_axis=0, concat_axis=0, tiled=True)  15.3 us
    pallas_call x1, Pallas kernels, expert(): pl.pallas_call(expert_kernel, out_shape=jax.ShapeDtypeStruct((rows, width...  14.1 us
    pallas_call x1, Pallas kernels, attend(): pl.pallas_call(attend_kernel, out_shape=jax.ShapeDtypeStruct((blocks, row...  11.8 us
    all_to_all x2, waiting for transfers between devices, swap(): return lax.all_to_all(x, 'sp', split_axis=0, concat_axis=0, tiled=True)  11 us
    pallas_call x1, Pallas kernels, project(): pl.pallas_call(project_kernel, out_shape=(jax.ShapeDtypeStruct((rows, wid...  5.65 us
    ppermute x3, starting transfers between devices, gather_shards(): lax.ppermute(x, 'dp', [(d, (d // 2 + k) % chips * 2 + d % 2) for d in ran...  4.51 us
  transfers between devices with their start and end apart: 9, of which 3 were waited for; matrix products, arithmetic and copies ran while one was open for 0% of the time, Pallas kernels for 6%

profile of v2, /device:TPU:0, one launch (start us, length us, event | category | flops | bytes accessed | tf_op | source)
XLA Modules:
  0.0 201.1 jit_solution(2319235942490451885)
XLA Ops:
  0.0 2.7 %pack.1 = bf16[16,400,128]{2,1,0:T(8,128)(2,1)} custom-call(bf16[1,256,1024]{2,1,0:T(8,128)(2,1)} %q_hbm.1, bf16[1,256,1024]{2,1,0:T(8,128)(2,1)} %k_hbm.1, bf16[1,256,1024]{2,1,0:T(8,128)(2,1)} %v_hbm.1, f32[16,256]{1,0:T(8,128)} %bitcast.35), custom_call_target="tpu_custom_call" | custom-call | tf_op jit(solution)/shard_map/pack/pallas_call | solution.py:76
  2.7 8.2 %all-to-all-start = ((bf16[16,400,128]{2,1,0:T(8,128)(2,1)}), bf16[16,400,128]{2,1,0:T(8,128)(2,1)S(1)}, u32[]{:S(2)}, u32[]{:S(2)}) async-start(bf16[16,400,128]{2,1,0:T(8,128)(2,1)} %pack.1), calls=%async_computation | async-start | bytes 3276800 | tf_op jit(solution)/shard_map/all_to_all | solution.py:401
  10.9 0.0 copy-start.7
  10.9 0.0 copy-start.8
  10.9 0.0 copy-start.4
  11.0 2.8 %collective-permute-start.2 = (bf16[1024,256]{1,0:T(8,128)(2,1)S(1)}, bf16[1024,256]{1,0:T(8,128)(2,1)}, u32[]{:S(2)}, u32[]{:S(2)}) collective-permute-start(bf16[1024,256]{1,0:T(8,128)(2,1)S(1)} %copy-done.1), channel_id=1, source_target_pairs={{0,6},{1,7},{2,0},{3,1},{4,2},{5,3},{6,4},{7,5},{8,14},{9,15},{10,... | collective-permute-start | bytes 1572872 | tf_op jit(solution)/shard_map/ppermute | solution.py:410
  13.8 0.8 collective-permute-start.1
  14.6 0.9 collective-permute-start
  15.5 20.5 %collective-permute-done.2.refs_5_ = bf16[1024,256]{1,0:T(8,128)(2,1)} collective-permute-done((bf16[1024,256]{1,0:T(8,128)(2,1)S(1)}, bf16[1024,256]{1,0:T(8,128)(2,1)}, u32[]{:S(2)}, u32[]{:S(2)}) %collective-permute-start.2) | collective-permute-done | bytes 524320 | tf_op jit(solution)/shard_map/ppermute | solution.py:410
  36.0 0.5 collective-permute-start.5
  36.5 3.3 %collective-permute-done.refs_3_ = bf16[1024,256]{1,0:T(8,128)(2,1)} collective-permute-done((bf16[1024,256]{1,0:T(8,128)(2,1)S(1)}, bf16[1024,256]{1,0:T(8,128)(2,1)}, u32[]{:S(2)}, u32[]{:S(2)}) %collective-permute-start) | collective-permute-done | bytes 524320 | tf_op jit(solution)/shard_map/ppermute | solution.py:410
  39.7 0.0 collective-permute-start.4
  39.7 11.8 %attend.1 = bf16[16,128,128]{2,1,0:T(8,128)(2,1)S(1)} custom-call(bf16[16,400,128]{2,1,0:T(8,128)(2,1)S(1)} %all-to-all-done.x_ref), custom_call_target="tpu_custom_call" | custom-call | flops 4294967296 | bytes 4000000 | tf_op jit(solution)/shard_map/attend/pallas_call | solution.py:208
  51.6 0.8 copy-done.2
  52.3 7.2 %all-to-all-start.1 = ((bf16[16,128,128]{2,1,0:T(8,128)(2,1)}), bf16[16,128,128]{2,1,0:T(8,128)(2,1)S(1)}, u32[]{:S(2)}, u32[]{:S(2)}) async-start(bf16[16,128,128]{2,1,0:T(8,128)(2,1)} %copy-done.2), calls=%async_computation.1 | async-start | bytes 1048576 | tf_op jit(solution)/shard_map/all_to_all | solution.py:401
  59.5 1.1 route_tables.1
  60.7 11.0 %all-to-all-done.1.refs_1_ = bf16[16,128,128]{2,1,0:T(8,128)(2,1)S(1)} async-done(((bf16[16,128,128]{2,1,0:T(8,128)(2,1)}), bf16[16,128,128]{2,1,0:T(8,128)(2,1)S(1)}, u32[]{:S(2)}, u32[]{:S(2)}) %all-to-all-start.1) | async-done | bytes 524320 | tf_op jit(solution)/shard_map/all_to_all | solution.py:401
  71.7 0.0 copy-start.11
  71.7 5.7 %project.1 = (bf16[256,2048]{1,0:T(8,128)(2,1)S(1)}, bf16[1024,2048]{1,0:T(8,128)(2,1)S(1)}) custom-call(s32[1]{0:T(128)} %bitcast.4.refs_0_, bf16[16,128,128]{2,1,0:T(8,128)(2,1)S(1)} %all-to-all-done.1.refs_1_, bf16[1024,256]{1,0:T(8,128)(2,1)S(1)} %copy-done.1, bf16[1024,256]{1,0:T(8,128)(2,1)} %collective-permute-done.refs_3_, ...), custom_call_target="tpu_custom_call" | custom-call | tf_op jit(solution)/shard_map/project/pallas_call | solution.py:316
  77.4 0.0 copy-start.10
  77.4 53.7 %all_to_all.20 = bf16[16,64,2048]{2,1,0:T(8,128)(2,1)S(1)} all-to-all(bf16[16,64,2048]{2,1,0:T(8,128)(2,1)S(1)} %bitcast.23), channel_id=1, replica_groups=mesh['sp'=16,'dp'=8] {'sp'}, dimensions={0} | all-to-all | bytes 8388608 | tf_op jit(solution)/shard_map/all_to_all | solution.py:401
  131.1 14.1 %expert.1 = bf16[1024,2048]{1,0:T(8,128)(2,1)S(1)} custom-call(bf16[1024,2048]{1,0:T(8,128)(2,1)S(1)} %bitcast.24, bf16[2048,1024]{1,0:T(8,128)(2,1)S(1)} %bitcast.32, bf16[2048,1024]{1,0:T(8,128)(2,1)S(1)} %bitcast.33, bf16[1024,2048]{1,0:T(8,128)(2,1)S(1)} %bitcast.34), custom_call_target="tpu_custom_call" | custom-call | flops 12884901888 | bytes 20000000 | tf_op jit(solution)/shard_map/expert/pallas_call | solution.py:358
  145.2 53.7 %all_to_all.21 = bf16[16,64,2048]{2,1,0:T(8,128)(2,1)S(1)} all-to-all(bf16[16,64,2048]{2,1,0:T(8,128)(2,1)S(1)} %bitcast.25), channel_id=1, replica_groups=mesh['sp'=16,'dp'=8] {'sp'}, dimensions={0} | all-to-all | bytes 8388608 | tf_op jit(solution)/shard_map/all_to_all | solution.py:401
  198.9 2.0 %finish.1 = bf16[256,2048]{1,0:T(8,128)(2,1)} custom-call(bf16[256,1024]{1,0:T(8,128)(2,1)S(1)} %get-tuple-element.9.c_ref, bf16[1024,2048]{1,0:T(8,128)(2,1)S(1)} %bitcast.22, bf16[256,2048]{1,0:T(8,128)(2,1)S(1)} %get-tuple-element.12.hid_ref, f32[1,2048]{1,0:T(1,128)S(1)} %bitcast.29), custom_call_target="tpu_custom_call" | custom-call | tf_op jit(solution)/shard_map/finish/pallas_call | solution.py:389
  (26 shorter events, 0.1 us)
Async XLA Ops:
  0.0 10.9 %copy-start.1 = (bf16[1024,256]{1,0:T(8,128)(2,1)S(1)}, bf16[1024,256]{1,0:T(8,128)(2,1)}, u32[]{:S(2)}) copy-start(bf16[1024,256]{1,0:T(8,128)(2,1)} %refs_2_.1) | copy-start | bytes 1572868
  2.7 37.1 %all-to-all-start = ((bf16[16,400,128]{2,1,0:T(8,128)(2,1)}), bf16[16,400,128]{2,1,0:T(8,128)(2,1)S(1)}, u32[]{:S(2)}, u32[]{:S(2)}) async-start(bf16[16,400,128]{2,1,0:T(8,128)(2,1)} %pack.1), calls=%async_computation | async-start | bytes 3276800 | tf_op jit(solution)/shard_map/all_to_all | solution.py:401
  10.9 48.6 %copy-start.6 = (s32[1,256,2]{1,2,0:T(2,128)S(1)}, s32[1,256,2]{1,2,0:T(2,128)}, u32[]{:S(2)}) copy-start(s32[1,256,2]{1,2,0:T(2,128)} %param.24) | copy-start | bytes 6148
  10.9 48.6 %copy-start.7 = (f32[1,256,2]{1,2,0:T(2,128)S(1)}, f32[1,256,2]{1,2,0:T(2,128)}, u32[]{:S(2)}) copy-start(f32[1,256,2]{1,2,0:T(2,128)} %param.26) | copy-start | bytes 6148
  10.9 48.6 %copy-start.8 = (f32[1,256]{1,0:T(1,128)S(1)}, f32[1,256]{1,0:T(1,128)}, u32[]{:S(2)}) copy-start(f32[1,256]{1,0:T(1,128)} %gs_ref.1) | copy-start | bytes 3076
  10.9 60.8 %copy-start = (bf16[1,256,2048]{2,1,0:T(8,128)(2,1)S(1)}, bf16[1,256,2048]{2,1,0:T(8,128)(2,1)}, u32[]{:S(2)}) copy-start(bf16[1,256,2048]{2,1,0:T(8,128)(2,1)} %param.15) | copy-start | bytes 3145732
  10.9 60.8 %copy-start.3 = (f32[2048]{0:T(1024)S(1)}, f32[2048]{0:T(1024)}, u32[]{:S(2)}) copy-start(f32[2048]{0:T(1024)} %param.21) | copy-start | bytes 24580
  10.9 60.8 %copy-start.4 = (f32[2048]{0:T(1024)S(1)}, f32[2048]{0:T(1024)}, u32[]{:S(2)}) copy-start(f32[2048]{0:T(1024)} %param.22) | copy-start | bytes 24580
  11.0 25.0 %collective-permute-start.2 = (bf16[1024,256]{1,0:T(8,128)(2,1)S(1)}, bf16[1024,256]{1,0:T(8,128)(2,1)}, u32[]{:S(2)}, u32[]{:S(2)}) collective-permute-start(bf16[1024,256]{1,0:T(8,128)(2,1)S(1)} %copy-done.1), channel_id=1, source_target_pairs={{0,6},{1,7},{2,0},{3,1},{4,2},{5,3},{6,4},{7,5},{8,14},{9,15},{10,... | collective-permute-start | bytes 1572872 | tf_op jit(solution)/shard_map/ppermute | solution.py:410
  13.8 22.2 %collective-permute-start.1 = (bf16[1024,256]{1,0:T(8,128)(2,1)S(1)}, bf16[1024,256]{1,0:T(8,128)(2,1)}, u32[]{:S(2)}, u32[]{:S(2)}) collective-permute-start(bf16[1024,256]{1,0:T(8,128)(2,1)S(1)} %copy-done.1), channel_id=1, source_target_pairs={{0,4},{1,5},{2,6},{3,7},{4,0},{5,1},{6,2},{7,3},{8,12},{9,13},{10,... | collective-permute-start | bytes 1572872 | tf_op jit(solution)/shard_map/ppermute | solution.py:410
  14.6 25.1 %collective-permute-start = (bf16[1024,256]{1,0:T(8,128)(2,1)S(1)}, bf16[1024,256]{1,0:T(8,128)(2,1)}, u32[]{:S(2)}, u32[]{:S(2)}) collective-permute-start(bf16[1024,256]{1,0:T(8,128)(2,1)S(1)} %copy-done.1), channel_id=1, source_target_pairs={{0,2},{1,3},{2,4},{3,5},{4,6},{5,7},{6,0},{7,1},{8,10},{9,11},{10,... | collective-permute-start | bytes 1572872 | tf_op jit(solution)/shard_map/ppermute | solution.py:410
  15.5 45.2 %collective-permute-start.3 = (bf16[1024,256]{1,0:T(8,128)(2,1)S(1)}, bf16[1024,256]{1,0:T(8,128)(2,1)}, u32[]{:S(2)}, u32[]{:S(2)}) collective-permute-start(bf16[1024,256]{1,0:T(8,128)(2,1)S(1)} %copy-done.1), channel_id=1, source_target_pairs={{0,1},{1,0},{2,3},{3,2},{4,5},{5,4},{6,7},{7,6},{8,9},{9,8},{10,11... | collective-permute-start | bytes 1572872 | tf_op jit(solution)/shard_map/ppermute | solution.py:411
  35.9 24.7 %collective-permute-start.6 = (bf16[1024,256]{1,0:T(8,128)(2,1)}, bf16[1024,256]{1,0:T(8,128)(2,1)}, u32[]{:S(2)}, u32[]{:S(2)}) collective-permute-start(bf16[1024,256]{1,0:T(8,128)(2,1)} %collective-permute-done.2.refs_5_), channel_id=1, source_target_pairs={{0,1},{1,0},{2,3},{3,2},{4,5},{5,4},{6,7},{7,6},{8,9},{9,8},{10,11... | collective-permute-start | bytes 1572872 | tf_op jit(solution)/shard_map/ppermute | solution.py:411
  36.0 24.7 %collective-permute-start.5 = (bf16[1024,256]{1,0:T(8,128)(2,1)}, bf16[1024,256]{1,0:T(8,128)(2,1)}, u32[]{:S(2)}, u32[]{:S(2)}) collective-permute-start(bf16[1024,256]{1,0:T(8,128)(2,1)} %collective-permute-done.1.refs_4_), channel_id=1, source_target_pairs={{0,1},{1,0},{2,3},{3,2},{4,5},{5,4},{6,7},{7,6},{8,9},{9,8},{10,11... | collective-permute-start | bytes 1572872 | tf_op jit(solution)/shard_map/ppermute | solution.py:411
  39.7 20.9 %collective-permute-start.4 = (bf16[1024,256]{1,0:T(8,128)(2,1)}, bf16[1024,256]{1,0:T(8,128)(2,1)}, u32[]{:S(2)}, u32[]{:S(2)}) collective-permute-start(bf16[1024,256]{1,0:T(8,128)(2,1)} %collective-permute-done.refs_3_), channel_id=1, source_target_pairs={{0,1},{1,0},{2,3},{3,2},{4,5},{5,4},{6,7},{7,6},{8,9},{9,8},{10,11... | collective-permute-start | bytes 1572872 | tf_op jit(solution)/shard_map/ppermute | solution.py:411
  51.5 0.8 copy-start.2
  52.3 19.4 %all-to-all-start.1 = ((bf16[16,128,128]{2,1,0:T(8,128)(2,1)}), bf16[16,128,128]{2,1,0:T(8,128)(2,1)S(1)}, u32[]{:S(2)}, u32[]{:S(2)}) async-start(bf16[16,128,128]{2,1,0:T(8,128)(2,1)} %copy-done.2), calls=%async_computation.1 | async-start | bytes 1048576 | tf_op jit(solution)/shard_map/all_to_all | solution.py:401
  71.7 59.4 %copy-start.11 = (bf16[1,1024,2048]{2,1,0:T(8,128)(2,1)S(1)}, bf16[1,1024,2048]{2,1,0:T(8,128)(2,1)}, u32[]{:S(2)}) copy-start(bf16[1,1024,2048]{2,1,0:T(8,128)(2,1)} %param.29) | copy-start | bytes 12582916
  77.4 53.7 %copy-start.9 = (bf16[1,2048,1024]{2,1,0:T(8,128)(2,1)S(1)}, bf16[1,2048,1024]{2,1,0:T(8,128)(2,1)}, u32[]{:S(2)}) copy-start(bf16[1,2048,1024]{2,1,0:T(8,128)(2,1)} %param.27) | copy-start | bytes 12582916
  77.4 53.7 %copy-start.10 = (bf16[1,2048,1024]{2,1,0:T(8,128)(2,1)S(1)}, bf16[1,2048,1024]{2,1,0:T(8,128)(2,1)}, u32[]{:S(2)}) copy-start(bf16[1,2048,1024]{2,1,0:T(8,128)(2,1)} %param.28) | copy-start | bytes 12582916
  145.2 53.7 %copy-start.5 = (f32[2048]{0:T(1024)S(1)}, f32[2048]{0:T(1024)}, u32[]{:S(2)}) copy-start(f32[2048]{0:T(1024)} %param.23) | copy-start | bytes 24580
